TPU v7x, 32 devices: a whole 2x2x4 slice. The times are simulated.
32 devices in a mesh: sp: 16 (over z, y, core), tp: 2 (over x).
Axes of the slice: x: 2, y: 2, z: 4, core: 2. Of those that a mesh axis runs over, the one named last changes fastest.
Arguments:
- query_content: bfloat16 [3072, 1024], P('sp'), may hold values from -6 to 6
- query_rotary: bfloat16 [3072, 512], P('sp'), may hold values from -8 to 8
- latents: bfloat16 [3072, 256], P(('sp', 'tp')), may hold values from -6 to 6
- key_rotary: bfloat16 [3072, 64], P(('sp', 'tp')), may hold values from -8 to 8
- latent_gain: float32 [256], replicated, may hold values from 0.1 to 1.9
- key_up: bfloat16 [256, 1024], P(None, 'tp'), may hold values from -0.375 to 0.375
- value_up: bfloat16 [256, 1024], P(None, 'tp'), may hold values from -0.375 to 0.375
- out_proj: bfloat16 [1024, 2048], P(None, 'tp'), may hold values from -2 to 2
- residual: bfloat16 [3072, 2048], P('sp', 'tp'), may hold values from -6 to 6
- mixer_gain: float32 [2048], replicated, may hold values from 0.1 to 1.9
- gate_proj: bfloat16 [2048, 5632], P('sp', 'tp'), may hold values from -0.125 to 0.125
- up_proj: bfloat16 [2048, 5632], P('sp', 'tp'), may hold values from -0.125 to 0.125
- down_proj: bfloat16 [5632, 2048], P('tp', 'sp'), may hold values from -0.078125 to 0.078125
Outputs:
- layer_out: bfloat16 [3072, 2048], P('sp', 'tp')
All inputs are finite; a program needn't handle non-finite values.
Results may differ from a plain program's by a relative error of at most 0.011.
Values may be sent and summed in bfloat16 or wider, within the bound.
A program may use at most 128 MiB of HBM per device.

v0:
```python
import math

import jax
import jax.numpy as jnp
from jax import lax
from jax.sharding import PartitionSpec as P

H = 8
DN = 128
DR = 64
DV = 128
SPAN = 64


epsilon = 1e-06
masked_score = -1e30
heads_per_step = 2


def norm_round(inputs, scales):
    widened = inputs.astype(jnp.float32)
    factor = lax.rsqrt(jnp.mean(widened * widened, axis=-1, keepdims=True) + epsilon)
    return (widened * factor * scales).astype(jnp.bfloat16)


def rotate(inputs, places):
    dimension = inputs.shape[-1]
    middle = dimension // 2
    inverse = 10000.0 ** (-jnp.arange(0, dimension, 2, dtype=jnp.float32) / dimension)
    angles = places.astype(jnp.float32)[:, None, None] * inverse[None, None, :]
    cosine_table = jnp.cos(angles)
    sine_table = jnp.sin(angles)
    widened = inputs.astype(jnp.float32)
    first_half = widened[..., :middle]
    second_half = widened[..., middle:]
    return jnp.concatenate(
        [
            first_half * cosine_table - second_half * sine_table,
            second_half * cosine_table + first_half * sine_table,
        ],
        axis=-1,
    ).astype(jnp.bfloat16)


def shards(
    query_content,
    query_rotary,
    latents,
    key_rotary,
    latent_gain,
    key_up,
    value_up,
    out_proj,
    residual,
    mixer_gain,
    gate_proj,
    up_proj,
    down_proj,
):
    query_rows = query_content.shape[0]
    tp_count = lax.axis_size("tp")
    sp_index = lax.axis_index("sp")
    tp_index = lax.axis_index("tp")
    latent_whole, turn_whole = (
        lax.all_gather(latents, "sp", axis=0, tiled=True),
        lax.all_gather(key_rotary, "sp", axis=0, tiled=True),
    )
    key_weights, value_weights = (
        lax.all_gather(key_up, "tp", axis=1, tiled=True),
        lax.all_gather(value_up, "tp", axis=1, tiled=True),
    )
    per_device = latents.shape[0]
    row_count = latent_whole.shape[0]
    position_index = jnp.arange(row_count, dtype=jnp.int32)
    key_places = (
        position_index // per_device * tp_count + tp_index
    ) * per_device + position_index % per_device
    query_places = sp_index * query_rows + jnp.arange(query_rows, dtype=jnp.int32)
    normed = norm_round(latent_whole, latent_gain)
    key_turned = rotate(turn_whole[:, None, :], key_places)[:, 0, :]
    query_turned = rotate(query_rotary.reshape(query_rows, H, DR), query_places)
    allowed = (key_places[None, :] // SPAN <= query_places[:, None] // SPAN)[:, None, :]
    groups = H // heads_per_step
    score_scale = 1.0 / math.sqrt(DN + DR)

    def by_group(inputs):
        shaped = inputs.reshape((inputs.shape[0], groups, heads_per_step) + inputs.shape[2:])
        return jnp.moveaxis(shaped, 1, 0)

    def weight_group(weights, width):
        return jnp.moveaxis(weights.reshape(weights.shape[0], groups, heads_per_step * width), 1, 0)

    def attend(inputs):
        contents, turned, key_weight, value_weight = inputs
        key_rows = jnp.dot(normed, key_weight, preferred_element_type=jnp.float32).astype(
            jnp.bfloat16
        )
        value_rows = jnp.dot(normed, value_weight, preferred_element_type=jnp.float32).astype(
            jnp.bfloat16
        )
        key_rows = key_rows.reshape(row_count, heads_per_step, DN)
        value_rows = value_rows.reshape(row_count, heads_per_step, DV)
        scores = (
            jnp.einsum("qhd,khd->qhk", contents, key_rows, preferred_element_type=jnp.float32)
            + jnp.einsum("qhr,kr->qhk", turned, key_turned, preferred_element_type=jnp.float32)
        ) * score_scale
        highest = jnp.max(jnp.where(allowed, scores, masked_score), axis=-1)
        weights = jnp.where(allowed, jnp.exp(scores - highest[..., None]), 0.0)
        weight_sum = jnp.sum(weights, axis=-1)
        weighted = jnp.einsum(
            "qhk,khv->qhv",
            weights.astype(jnp.bfloat16),
            value_rows,
            preferred_element_type=jnp.float32,
        )
        return (highest, weight_sum, weighted)

    highest, weight_sum, weighted = lax.map(
        attend,
        (
            by_group(query_content.reshape(query_rows, H, DN)),
            by_group(query_turned),
            weight_group(key_weights, DN),
            weight_group(value_weights, DV),
        ),
    )
    highest = jnp.moveaxis(highest, 0, 1).reshape(query_rows, H)
    weight_sum = jnp.moveaxis(weight_sum, 0, 1).reshape(query_rows, H)
    weighted = jnp.moveaxis(weighted, 0, 1).reshape(query_rows, H, DV)
    high_parts, sum_parts, acc_parts = (
        lax.all_to_all(highest[None], "tp", split_axis=2, concat_axis=0, tiled=True),
        lax.all_to_all(weight_sum[None], "tp", split_axis=2, concat_axis=0, tiled=True),
        lax.all_to_all(weighted[None], "tp", split_axis=2, concat_axis=0, tiled=True),
    )
    overall = jnp.max(high_parts, axis=0)
    factor = jnp.exp(high_parts - overall)
    own_heads = (
        jnp.sum(factor[..., None] * acc_parts, axis=0)
        / jnp.sum(factor * sum_parts, axis=0)[..., None]
    ).astype(jnp.bfloat16)
    attended = lax.all_gather(own_heads.reshape(query_rows, -1), "tp", axis=1, tiled=True)
    mixed_rows = (
        residual.astype(jnp.float32)
        + jnp.dot(attended, out_proj, preferred_element_type=jnp.float32)
    ).astype(jnp.bfloat16)
    whole_rows = lax.all_gather(mixed_rows, "tp", axis=1, tiled=True)
    normed_rows = norm_round(whole_rows, mixer_gain)
    gate_whole, up_whole, down_whole = (
        lax.all_gather(gate_proj, "sp", axis=0, tiled=True),
        lax.all_gather(up_proj, "sp", axis=0, tiled=True),
        lax.all_gather(down_proj, "sp", axis=1, tiled=True),
    )
    hidden = (
        jax.nn.silu(jnp.dot(normed_rows, gate_whole, preferred_element_type=jnp.float32))
        * jnp.dot(normed_rows, up_whole, preferred_element_type=jnp.float32)
    ).astype(jnp.bfloat16)
    partial_value = jnp.dot(hidden, down_whole, preferred_element_type=jnp.float32)
    mixer_out = lax.psum_scatter(
        partial_value.astype(jnp.bfloat16), "tp", scatter_dimension=1, tiled=True
    ).astype(jnp.float32)
    return (mixed_rows.astype(jnp.float32) + mixer_out).astype(jnp.bfloat16)


def solution(mesh):
    return jax.shard_map(
        shards,
        mesh=mesh,
        in_specs=(
            P("sp", None),
            P("sp", None),
            P(("sp", "tp"), None),
            P(("sp", "tp"), None),
            P(),
            P(None, "tp"),
            P(None, "tp"),
            P(None, "tp"),
            P("sp", "tp"),
            P(),
            P("sp", "tp"),
            P("sp", "tp"),
            P("tp", "sp"),
        ),
        out_specs=P("sp", "tp"),
        check_vma=False,
    )
```

profile of v0, /device:TPU:0, one launch (start us, length us, event | category | flops | bytes accessed | tf_op | source)
XLA Modules:
  0.0 344.1 jit_solution(9757304870552600955)
XLA Ops:
  9.0 25.1 %all-gather = bf16[16,96,64]{1,2,0:T(8,128)(2,1)S(1)} all-gather(bf16[1,96,64]{1,2,0:T(8,128)(2,1)S(1)} %bitcast.148), channel_id=1, replica_groups=mesh['sp'=16,'tp'=2] {'sp'}, dimensions={0}, use_global_device_ids=true | all-gather | bytes 208896 | tf_op jit(solution)/shard_map/all_gather | solution.py:66
  37.4 1.3 reshape_reshape.3
  39.8 9.4 %all_gather.27 = bf16[256,1024]{0,1:T(8,128)(2,1)} all-gather(bf16[256,512]{0,1:T(8,128)(2,1)S(1)} %copy.40), channel_id=1, replica_groups=mesh['sp'=16,'tp'=2] {'tp'}, dimensions={1}, use_global_device_ids=true | all-gather | bytes 786432 | tf_op jit(solution)/shard_map/all_gather | solution.py:69
  49.2 8.5 %all_gather.30 = bf16[256,1024]{0,1:T(8,128)(2,1)} all-gather(bf16[256,512]{0,1:T(8,128)(2,1)S(1)} %copy.43), channel_id=1, replica_groups=mesh['sp'=16,'tp'=2] {'tp'}, dimensions={1}, use_global_device_ids=true | all-gather | bytes 786432 | tf_op jit(solution)/shard_map/all_gather | solution.py:70
  57.7 24.8 %all_gather.28 = bf16[1536,256]{1,0:T(8,128)(2,1)S(1)} all-gather(bf16[96,256]{1,0:T(8,128)(2,1)S(1)} %copy-done.4), channel_id=1, replica_groups=mesh['sp'=16,'tp'=2] {'sp'}, dimensions={0}, use_global_device_ids=true | all-gather | bytes 835584 | tf_op jit(solution)/shard_map/all_gather | solution.py:65
  83.9 28.5 %while.15 = (s32[]{:T(128)}, f32[4,192,2]{1,2,0:T(2,128)S(1)}, f32[4,192,2]{1,2,0:T(2,128)S(1)}, f32[4,192,2,128]{3,1,2,0:T(8,128)}, bf16[4,256,256]{1,2,0:T(8,1...) while((s32[]{:T(128)}, f32[4,192,2]{1,2,0:T(2,128)S(1)}, ...), condition=%wide.region_4.5_spmd.clone, body=%wide.region_1.4_spmd.clone.sunk | while | flops 787119360 | bytes 18733956 | solution.py:118
  83.9 1.3 convolution_convert_fusion.5
  86.0 1.7 select_reduce_fusion.2
  87.7 1.3 convolution_convert_fusion.6
  89.0 1.2 fusion.96
  91.0 1.3 convolution_convert_fusion.5
  93.1 1.7 select_reduce_fusion.2
  94.8 1.3 convolution_convert_fusion.6
  98.1 1.3 convolution_convert_fusion.5
  100.2 1.7 select_reduce_fusion.2
  101.9 1.3 convolution_convert_fusion.6
  105.2 1.3 convolution_convert_fusion.5
  107.3 1.7 select_reduce_fusion.2
  109.1 1.3 convolution_convert_fusion.6
  113.0 3.2 all-to-all-start
  116.2 3.8 %all-to-all-done = f32[1,192,8]{1,0,2:T(1,128)S(1)} async-done(((f32[1,192,8]{1,0,2:T(1,128)}), f32[1,192,8]{1,0,2:T(1,128)S(1)}, u32[]{:S(2)}, u32[]{:S(2)}) %all-to-all-start) | async-done | bytes 6176 | tf_op jit(solution)/shard_map/all_to_all | solution.py:131
  120.0 6.1 %all_to_all.54 = f32[1,192,8]{1,0,2:T(1,128)S(1)} all-to-all(f32[1,192,8]{1,0,2:T(1,128)S(1)} %broadcast_in_dim_reshape.11), channel_id=1, replica_groups=mesh['sp'=16,'tp'=2] {'tp'}, dimensions={2} | all-to-all | bytes 12288 | tf_op jit(solution)/shard_map/all_to_all | solution.py:132
  126.2 3.5 %all-to-all-start.1 = ((f32[1,192,8,128]{3,1,0,2:T(8,128)}), f32[1,192,8,128]{3,1,0,2:T(8,128)S(1)}, u32[]{:S(2)}, u32[]{:S(2)}) async-start(f32[1,192,8,128]{3,1,0,2:T(8,128)} %bitcast.142), calls=%async_computation.1 | async-start | bytes 1572864 | tf_op jit(solution)/shard_map/all_to_all | solution.py:133
  129.8 9.2 %all-to-all-done.1 = f32[1,192,8,128]{3,1,0,2:T(8,128)S(1)} async-done(((f32[1,192,8,128]{3,1,0,2:T(8,128)}), f32[1,192,8,128]{3,1,0,2:T(8,128)S(1)}, u32[]{:S(2)}, u32[]{:S(2)}) %all-to-all-start.1) | async-done | bytes 786464 | tf_op jit(solution)/shard_map/all_to_all | solution.py:133
  139.4 6.3 %all_gather.31 = bf16[192,1024]{1,0:T(8,128)(2,1)S(1)} all-gather(bf16[192,512]{1,0:T(8,128)(2,1)S(1)} %copy_bitcast_fusion.2), channel_id=1, replica_groups=mesh['sp'=16,'tp'=2] {'tp'}, dimensions={1}, use_global_device_ids=true | all-gather | bytes 589824 | tf_op jit(solution)/shard_map/all_gather | solution.py:141
  146.4 8.6 %all_gather.32 = bf16[192,2048]{1,0:T(8,128)(2,1)S(1)} all-gather(bf16[192,1024]{1,0:T(8,128)(2,1)S(1)} %fusion.34), channel_id=1, replica_groups=mesh['sp'=16,'tp'=2] {'tp'}, dimensions={1}, use_global_device_ids=true | all-gather | bytes 1179648 | tf_op jit(solution)/shard_map/all_gather | solution.py:146
  155.3 8.2 %fusion.41 = f32[192,2816]{1,0:T(8,128)} fusion(bf16[2048,2816]{1,0:T(8,128)(2,1)} %all-gather.5.cloned.1.call-done, bf16[192,2048]{1,0:T(8,128)(2,1)S(1)} %all_gather.32, f32[2048]{0:T(1024)S(1)} %copy-done.9, f32[192]{0:T(256)S(1)} %add_rsqrt_fusion.1), kind=kOutput, calls=%fused_computation.59 | convolution fusion | flops 2216165376 | bytes 14492416 | tf_op jit(solution)/shard_map/dot_general | solution.py:154
  163.5 45.1 %all-gather.7.cloned.1.call-done = bf16[2048,2816]{1,0:T(8,128)(2,1)} async-done(((bf16[128,2816]{1,0:T(8,128)(2,1)}), bf16[2048,2816]{1,0:T(8,128)(2,1)}) %all-gather.7.cloned.1.call-update) | async-done | bytes 11534352 | tf_op jit(solution)/shard_map/all_gather | solution.py:150
  208.6 97.3 %all-gather.9.cloned.1.call-done = bf16[2816,2048]{1,0:T(8,128)(2,1)} async-done(((bf16[2816,128]{1,0:T(8,128)(2,1)}), bf16[2816,2048]{1,0:T(8,128)(2,1)}) %all-gather.9.cloned.1.call-update) | async-done | bytes 11534352 | tf_op jit(solution)/shard_map/all_gather | solution.py:151
  306.0 13.9 %convolution_convert_fusion.2 = bf16[192,2048]{1,0:T(8,128)(2,1)} fusion(bf16[2816,2048]{1,0:T(8,128)(2,1)} %all-gather.9.cloned.1.call-done, bf16[2048,2816]{1,0:T(8,128)(2,1)} %all-gather.7.cloned.1.call-done, f32[192,2816]{1,0:T(8,128)} %fusion.41, bf16[192,2048]{1,0:T(8,128)(2,1)S(1)} %all_gather.32, f32[2048]{0:T(1024)S(1)} %copy-done.9, ...), kind=kOutput, calls=%fused_computation.34 | convolution fusion | flops 4434395136 | bytes 26813184 | tf_op jit(solution)/shard_map/dot_general | solution.py:157
  319.8 15.8 %reduce-scatter.2.cloned.1.call-done = bf16[192,1024]{1,0:T(8,128)(2,1)} async-done(((bf16[192,2048]{1,0:T(8,128)(2,1)}), bf16[192,1024]{1,0:T(8,128)(2,1)}) %reduce-scatter.2.cloned.1.call-update) | async-done | bytes 393232 | tf_op jit(solution)/shard_map/reduce_scatter | solution.py:158
  335.7 1.9 add_convert_fusion
  (83 shorter events, 19.8 us)
Async XLA Ops:
  6.5 139.3 %copy-start = (bf16[1024,1024]{1,0:T(8,128)(2,1)S(1)}, bf16[1024,1024]{1,0:T(8,128)(2,1)}, u32[]{:S(2)}) copy-start(bf16[1024,1024]{1,0:T(8,128)(2,1)} %param.22) | copy-start | bytes 6291460
  6.5 2.2 copy-start.3
  6.5 2.4 copy-start.5
  6.5 148.7 %all-gather.5.cloned.1.call-start = ((), (), s32[]{:S(2)}) async-start(), calls=%async_computation.4 | async-start | bytes 12255232 | tf_op jit(solution)/shard_map/all_gather | solution.py:149
  7.3 201.4 %all-gather.7.cloned.1.call-start = ((), (), s32[]{:S(2)}) async-start(), calls=%async_computation.5 | async-start | bytes 12255232 | tf_op jit(solution)/shard_map/all_gather | solution.py:150
  8.0 298.0 %all-gather.9.cloned.1.call-start = ((), (), s32[]{:S(2)}) async-start(), calls=%async_computation.6 | async-start | bytes 12255232 | tf_op jit(solution)/shard_map/all_gather | solution.py:151
  38.6 19.0 %copy-start.4 = (bf16[96,256]{1,0:T(8,128)(2,1)S(1)}, bf16[96,256]{1,0:T(8,128)(2,1)}, u32[]{:S(2)}) copy-start(bf16[96,256]{1,0:T(8,128)(2,1)} %param.17) | copy-start | bytes 147460
  38.9 43.8 %copy-start.1 = (f32[1536,1,64]{0,2,1:T(8,128)S(1)}, f32[1536,1,64]{0,2,1:T(8,128)}, u32[]{:S(2)}) copy-start(f32[1536,1,64]{0,2,1:T(8,128)} %reshape.384) | copy-start | bytes 1179652
  39.7 43.8 %copy-start.8 = (f32[256]{0:T(256)S(1)}, f32[256]{0:T(256)}, u32[]{:S(2)}) copy-start(f32[256]{0:T(256)} %param.19) | copy-start | bytes 3076
  57.7 26.2 %copy-start.6 = (f32[4,192,2]{1,2,0:T(2,128)S(1)}, f32[4,192,2]{1,2,0:T(2,128)}, u32[]{:S(2)}) copy-start(f32[4,192,2]{1,2,0:T(2,128)} %custom-call) | copy-start | bytes 18436
  57.7 26.2 %copy-start.7 = (f32[4,192,2]{1,2,0:T(2,128)S(1)}, f32[4,192,2]{1,2,0:T(2,128)}, u32[]{:S(2)}) copy-start(f32[4,192,2]{1,2,0:T(2,128)} %custom-call.1) | copy-start | bytes 18436
  112.4 33.4 %copy-start.2 = (bf16[192,1024]{1,0:T(8,128)(2,1)S(1)}, bf16[192,1024]{1,0:T(8,128)(2,1)}, u32[]{:S(2)}) copy-start(bf16[192,1024]{1,0:T(8,128)(2,1)} %param.23) | copy-start | bytes 1179652
  113.0 7.0 %all-to-all-start = ((f32[1,192,8]{1,0,2:T(1,128)}), f32[1,192,8]{1,0,2:T(1,128)S(1)}, u32[]{:S(2)}, u32[]{:S(2)}) async-start(f32[1,192,8]{1,0,2:T(1,128)} %broadcast_in_dim_reshape.9), calls=%async_computation | async-start | bytes 16384 | tf_op jit(solution)/shard_map/all_to_all | solution.py:131
  126.2 12.8 %all-to-all-start.1 = ((f32[1,192,8,128]{3,1,0,2:T(8,128)}), f32[1,192,8,128]{3,1,0,2:T(8,128)S(1)}, u32[]{:S(2)}, u32[]{:S(2)}) async-start(f32[1,192,8,128]{3,1,0,2:T(8,128)} %bitcast.142), calls=%async_computation.1 | async-start | bytes 1572864 | tf_op jit(solution)/shard_map/all_to_all | solution.py:133
  129.7 206.0 %reduce-scatter.2.cloned.1.call-start = ((), (), s32[]{:S(2)}) async-start(), calls=%async_computation.7 | async-start | bytes 1179648 | tf_op jit(solution)/shard_map/reduce_scatter | solution.py:158
  145.8 9.5 %copy-start.9 = (f32[2048]{0:T(1024)S(1)}, f32[2048]{0:T(1024)}, u32[]{:S(2)}) copy-start(f32[2048]{0:T(1024)} %param.24) | copy-start | bytes 24580
Sparse Core Ops, SparseCore 0:
  9.6 104.4 all-gather.4
  116.4 92.2 all-gather.6
  210.8 95.1 all-gather.8
  320.0 15.6 reduce-scatter.1
where the time goes:
time: 345 us; the launch traced here: 344 us
  waiting for transfers between devices  173 us (50%)
  blocking collectives  88.8 us (26%)
  matrix products  46.8 us (14%)
  between operations  13.4 us (4%)
  other arithmetic  8.88 us (3%)
  starting transfers between devices  6.88 us (2%)
  local copies, waits for them, and re-layouts  5.74 us (2%)
    all_gather x1, waiting for transfers between devices, shards(): lax.all_gather(down_proj, 'sp', axis=1, tiled=True)  97.3 us
    all_gather x1, waiting for transfers between devices, shards(): lax.all_gather(up_proj, 'sp', axis=0, tiled=True)  45.1 us
    all_gather x1, blocking collectives, shards(): lax.all_gather(key_rotary, 'sp', axis=0, tiled=True)  25.1 us
    all_gather x1, blocking collectives, shards(): lax.all_gather(latents, 'sp', axis=0, tiled=True)  24.8 us
    reduce_scatter x1, waiting for transfers between devices, shards(): lax.psum_scatter(partial_value.astype(jnp.bfloat16), 'tp', scatter_dimens...  15.8 us
    dot_general x1, matrix products, shards(): jnp.dot(hidden, down_whole, preferred_element_type=jnp.float32)  13.9 us
    all_gather x1, blocking collectives, shards(): lax.all_gather(key_up, 'tp', axis=1, tiled=True)  9.45 us
    all_to_all x1, waiting for transfers between devices, shards(): lax.all_to_all(weighted[None], 'tp', split_axis=2, concat_axis=0, tiled=T...  9.2 us
  transfers between devices with their start and end apart: 6, of which 5 were waited for; matrix products, arithmetic and copies ran while one was open for 13% of the time, Pallas kernels for 0%

commit v1 on v0

v1 whole, which is shorter than its diff:
```python
import math

import jax
import jax.numpy as jnp
from jax import lax
from jax.sharding import Mesh, PartitionSpec as P

H = 8
DN = 128
DR = 64
DV = 128
SPAN = 64


epsilon = 1e-06
masked_score = -1e30
SP = ("g", "r")


def norm_round(inputs, scales):
    widened = inputs.astype(jnp.float32)
    factor = lax.rsqrt(jnp.mean(widened * widened, axis=-1, keepdims=True) + epsilon)
    return (widened * factor * scales).astype(jnp.bfloat16)


def rotate(inputs, places):
    dimension = inputs.shape[-1]
    middle = dimension // 2
    inverse = 10000.0 ** (-jnp.arange(0, dimension, 2, dtype=jnp.float32) / dimension)
    angles = places.astype(jnp.float32)[:, None, None] * inverse[None, None, :]
    cosine_table = jnp.cos(angles)
    sine_table = jnp.sin(angles)
    widened = inputs.astype(jnp.float32)
    first_half = widened[..., :middle]
    second_half = widened[..., middle:]
    return jnp.concatenate(
        [
            first_half * cosine_table - second_half * sine_table,
            second_half * cosine_table + first_half * sine_table,
        ],
        axis=-1,
    ).astype(jnp.bfloat16)


def shards(
    query_content,
    query_rotary,
    latents,
    key_rotary,
    latent_gain,
    key_up,
    value_up,
    out_proj,
    residual,
    mixer_gain,
    gate_proj,
    up_proj,
    down_proj,
):
    query_rows = query_content.shape[0]
    tp_count = lax.axis_size("tp")
    members = lax.axis_size("r")
    sp_index = lax.axis_index(SP)
    tp_index = lax.axis_index("tp")
    rank = latents.shape[1]
    heads = H // tp_count

    own_keys = jnp.concatenate([latents, key_rotary], axis=1)
    all_keys = lax.all_gather(own_keys, SP + ("tp",), axis=0, tiled=True)
    row_count = all_keys.shape[0]

    def pieces(weights):
        rows, columns = weights.shape
        shaped = weights.reshape(rows, members, columns // members)
        return jnp.swapaxes(shaped, 0, 1)

    gate_up = jnp.concatenate([pieces(gate_proj), pieces(up_proj)], axis=2)
    down = pieces(down_proj.T)
    gate_up = lax.all_to_all(gate_up, "r", split_axis=0, concat_axis=0, tiled=True)
    down = lax.all_to_all(down, "r", split_axis=0, concat_axis=0, tiled=True)
    gate_up = lax.all_gather(
        gate_up.reshape(-1, gate_up.shape[-1]), "g", axis=0, tiled=True
    )
    down = lax.all_gather(down.reshape(-1, down.shape[-1]), "g", axis=0, tiled=True)

    key_places = jnp.arange(row_count, dtype=jnp.int32)
    query_places = sp_index * query_rows + jnp.arange(query_rows, dtype=jnp.int32)
    normed = norm_round(all_keys[:, :rank], latent_gain)
    key_turned = rotate(all_keys[:, None, rank:], key_places)[:, 0, :]
    own_rotary = lax.dynamic_slice_in_dim(query_rotary, tp_index * heads * DR, heads * DR, 1)
    own_content = lax.dynamic_slice_in_dim(query_content, tp_index * heads * DN, heads * DN, 1)
    query_turned = rotate(own_rotary.reshape(query_rows, heads, DR), query_places)
    allowed = key_places[None, :] // SPAN <= query_places[:, None] // SPAN
    score_scale = 1.0 / math.sqrt(DN + DR)
    key_rows = jnp.dot(normed, key_up, preferred_element_type=jnp.float32).astype(jnp.bfloat16)
    value_rows = jnp.dot(normed, value_up, preferred_element_type=jnp.float32).astype(jnp.bfloat16)
    outs = []
    for h in range(heads):
        k = jnp.concatenate([key_rows[:, h * DN : (h + 1) * DN], key_turned], axis=1)
        q = jnp.concatenate(
            [own_content[:, h * DN : (h + 1) * DN], query_turned[:, h, :]], axis=1
        )
        scores = lax.dot_general(
            q, k, (((1,), (1,)), ((), ())), preferred_element_type=jnp.float32
        )
        scores = jnp.where(allowed, scores * score_scale, masked_score)
        highest = jnp.max(scores, axis=-1, keepdims=True)
        weights = jnp.where(allowed, jnp.exp(scores - highest), 0.0)
        weight_sum = jnp.sum(weights, axis=-1, keepdims=True)
        weighted = jnp.dot(
            weights.astype(jnp.bfloat16),
            value_rows[:, h * DV : (h + 1) * DV],
            preferred_element_type=jnp.float32,
        )
        outs.append((weighted / weight_sum).astype(jnp.bfloat16))
    own_heads = jnp.concatenate(outs, axis=1)
    attended = lax.all_gather(own_heads, "tp", axis=1, tiled=True)
    mixed_rows = (
        residual.astype(jnp.float32)
        + jnp.dot(attended, out_proj, preferred_element_type=jnp.float32)
    ).astype(jnp.bfloat16)
    whole_rows = lax.all_gather(mixed_rows, "tp", axis=1, tiled=True)
    normed_rows = norm_round(whole_rows, mixer_gain)
    group_rows = lax.all_gather(normed_rows, "r", axis=0, tiled=True)
    both = jnp.dot(group_rows, gate_up, preferred_element_type=jnp.float32)
    units = both.shape[1] // 2
    hidden = (jax.nn.silu(both[:, :units]) * both[:, units:]).astype(jnp.bfloat16)
    partial_value = lax.dot_general(
        hidden, down, (((1,), (1,)), ((), ())), preferred_element_type=jnp.float32
    ).astype(jnp.bfloat16)
    mixer_out = lax.psum_scatter(partial_value, "r", scatter_dimension=0, tiled=True)
    mixer_out = lax.psum_scatter(mixer_out, "tp", scatter_dimension=1, tiled=True)
    return (mixed_rows.astype(jnp.float32) + mixer_out.astype(jnp.float32)).astype(jnp.bfloat16)


def solution(mesh):
    sp_count, tp_count = mesh.shape["sp"], mesh.shape["tp"]
    members = math.gcd(sp_count, 4)
    grouped = Mesh(
        mesh.devices.reshape(sp_count // members, members, tp_count), SP + ("tp",)
    )
    return jax.shard_map(
        shards,
        mesh=grouped,
        in_specs=(
            P(SP, None),
            P(SP, None),
            P(SP + ("tp",), None),
            P(SP + ("tp",), None),
            P(),
            P(None, "tp"),
            P(None, "tp"),
            P(None, "tp"),
            P(SP, "tp"),
            P(),
            P(SP, "tp"),
            P(SP, "tp"),
            P("tp", SP),
        ),
        out_specs=P(SP, "tp"),
        check_vma=False,
    )
```

time: 345 us -> 392 us (1.14)
  waiting for transfers between devices: 173 us -> 256 us
  blocking collectives: 88.8 us -> 69.3 us
  matrix products: 46.8 us -> 27.6 us
  local copies, waits for them, and re-layouts: 5.74 us -> 12.8 us
  starting transfers between devices: 6.88 us -> 0.24 us
    all_gather x5 -> x1, blocking collectives: 74.1 us -> 7.88 us  [shards(): attended = lax.all_gather(own_heads, 'tp', axis=1, tiled=True)]
    all_gather x3 -> x4, waiting for transfers between devices: 142 us -> 200 us  [the longest x1 93.7 us: shards(): lax.all_gather(gate_up.reshape(-1, gate_up.shape[-1]), 'g', axis=0, tiled...]
    all_to_all x1 -> x2, blocking collectives: 6.14 us -> 50.2 us  [the longest x1 35.8 us: shards(): lax.all_to_all(gate_up, 'r', split_axis=0, concat_axis=0, tiled=True)]
    reduce_scatter x1 -> x2, waiting for transfers between devices: 15.8 us -> 56.3 us  [the longest x1 36.7 us: shards(): lax.psum_scatter(partial_value, 'r', scatter_dimension=0, tiled=True)]
    dot_general x22 -> x12, matrix products: 46.2 us -> 27 us  [the longest x1 9.74 us: shards(): both = jnp.dot(group_rows, gate_up, preferred_element_type=jnp.float32)]
    all_to_all x2 -> x0, waiting for transfers between devices: 13 us -> none  [the longest x1 9.2 us: shards(): lax.all_to_all(weighted[None], 'tp', split_axis=2, concat_axis=0, tiled=T...]
    all_to_all x2 -> x0, starting transfers between devices: 6.76 us -> none  [the longest x1 3.53 us: shards(): lax.all_to_all(weighted[None], 'tp', split_axis=2, concat_axis=0, tiled=T...]
  transfers between devices with their start and end apart: 6 -> 6, of which waited for: 5 -> 5; matrix products, arithmetic and copies ran while one was open for 13% -> 5% of each run, Pallas kernels for 0% -> 0%
where the time goes in v1:
time: 392 us; the launch traced here: 391 us
  waiting for transfers between devices  256 us (65%)
  blocking collectives  69.3 us (18%)
  matrix products  27.6 us (7%)
  between operations  13.9 us (4%)
  local copies, waits for them, and re-layouts  12.8 us (3%)
  other arithmetic  10.8 us (3%)
    all_gather x1, waiting for transfers between devices, shards(): lax.all_gather(gate_up.reshape(-1, gate_up.shape[-1]), 'g', axis=0, tiled...  93.7 us
    all_gather x1, waiting for transfers between devices, shards(): all_keys = lax.all_gather(own_keys, SP + ('tp',), axis=0, tiled=True)  57.3 us
    all_gather x1, waiting for transfers between devices, shards(): lax.all_gather(down.reshape(-1, down.shape[-1]), 'g', axis=0, tiled=True)  49.1 us
    reduce_scatter x1, waiting for transfers between devices, shards(): lax.psum_scatter(partial_value, 'r', scatter_dimension=0, tiled=True)  36.7 us
    all_to_all x1, blocking collectives, shards(): lax.all_to_all(gate_up, 'r', split_axis=0, concat_axis=0, tiled=True)  35.8 us
    reduce_scatter x1, waiting for transfers between devices, shards(): lax.psum_scatter(mixer_out, 'tp', scatter_dimension=1, tiled=True)  19.6 us
    all_to_all x1, blocking collectives, shards(): down = lax.all_to_all(down, 'r', split_axis=0, concat_axis=0, tiled=True)  14.4 us
    all_gather x1, blocking collectives, shards(): whole_rows = lax.all_gather(mixed_rows, 'tp', axis=1, tiled=True)  11.2 us
  transfers between devices with their start and end apart: 6, of which 5 were waited for; matrix products, arithmetic and copies ran while one was open for 5% of the time, Pallas kernels for 0%

profile of v1, /device:TPU:0, one launch (start us, length us, event | category | flops | bytes accessed | tf_op | source)
XLA Modules:
  0.0 391.0 jit_solution(2140965674458963059)
XLA Ops:
  6.6 1.0 copy.29
  7.5 1.4 pad_maximum_fusion.14
  9.1 0.9 constant_dynamic-slice_fusion.3
  10.4 0.7 copy.28
  11.2 0.7 copy.31
  11.9 0.7 copy.32
  12.8 57.3 %all-gather.5.cloned.1.call-done = bf16[3072,320]{1,0:T(8,128)(2,1)} async-done(((bf16[96,320]{1,0:T(8,128)(2,1)}), bf16[3072,320]{1,0:T(8,128)(2,1)}) %all-gather.5.cloned.1.call-update) | async-done | bytes 1966096 | tf_op jit(solution)/shard_map/all_gather | solution.py:69
  70.1 1.9 fusion
  72.1 2.6 convolution_convert_fusion.1
  74.6 1.8 fusion.102
  76.7 1.6 fusion.69
  80.7 0.7 fusion.106
  82.5 2.0 fusion.4
  84.6 1.7 convolution_convert_fusion
  87.7 0.7 fusion.45
  88.4 0.7 fusion.42
  89.1 7.9 %all_gather.19 = bf16[192,1024]{1,0:T(8,128)(2,1)S(1)} all-gather(bf16[192,512]{1,0:T(8,128)(2,1)S(1)} %pad_maximum_fusion.13), channel_id=1, replica_groups=mesh['g'=4,'r'=4,'tp'=2] {'tp'}, dimensions={1}, use_global_device_ids=true | all-gather | bytes 589824 | tf_op jit(solution)/shard_map/all_gather | solution.py:117
  97.6 0.7 copy-done.1
  98.3 11.2 %all_gather.20 = bf16[192,2048]{1,0:T(8,128)(2,1)S(1)} all-gather(bf16[192,1024]{1,0:T(8,128)(2,1)S(1)} %fusion.15), channel_id=1, replica_groups=mesh['g'=4,'r'=4,'tp'=2] {'tp'}, dimensions={1}, use_global_device_ids=true | all-gather | bytes 1179648 | tf_op jit(solution)/shard_map/all_gather | solution.py:122
  109.7 1.1 fusion.14
  111.3 1.5 copy.35
  112.9 35.8 %all_to_all.10 = bf16[4,128,1408]{1,2,0:T(8,128)(2,1)S(1)} all-to-all(bf16[4,128,1408]{1,2,0:T(8,128)(2,1)S(1)} %pad_maximum_fusion.8), channel_id=1, replica_groups=mesh['g'=4,'r'=4,'tp'=2] {'r'}, dimensions={0} | all-to-all | bytes 2883584 | tf_op jit(solution)/shard_map/all_to_all | solution.py:79
  148.7 1.5 copy.36
  150.3 14.4 %all_to_all.11 = bf16[4,128,704]{1,2,0:T(8,128)(2,1)S(1)} all-to-all(bf16[4,128,704]{1,2,0:T(8,128)(2,1)} %bitcast.44), channel_id=1, replica_groups=mesh['g'=4,'r'=4,'tp'=2] {'r'}, dimensions={0} | all-to-all | bytes 1441792 | tf_op jit(solution)/shard_map/all_to_all | solution.py:80
  164.7 0.9 copy_bitcast_fusion
  165.8 93.7 %all-gather.9.cloned.1.call-done = bf16[2048,1408]{1,0:T(8,128)(2,1)} async-done(((bf16[512,1408]{1,0:T(8,128)(2,1)}), bf16[2048,1408]{1,0:T(8,128)(2,1)}) %all-gather.9.cloned.1.call-update) | async-done | bytes 5767184 | tf_op jit(solution)/shard_map/all_gather | solution.py:81
  259.5 9.7 %fusion.107 = f32[768,1408]{1,0:T(8,128)} fusion(bf16[768,2048]{1,0:T(8,128)(2,1)} %all-gather.7.cloned.1.call-done, bf16[2048,1408]{1,0:T(8,128)(2,1)} %all-gather.9.cloned.1.call-done), kind=kOutput, calls=%fused_computation.150 | convolution fusion | flops 4429185024 | bytes 13238272 | tf_op jit(solution)/shard_map/dot_general | solution.py:125
  269.2 49.1 %all-gather.11.cloned.1.call-done = bf16[2048,704]{0,1:T(8,128)(2,1)} async-done(((bf16[512,704]{0,1:T(8,128)(2,1)}), bf16[2048,704]{0,1:T(8,128)(2,1)}) %all-gather.11.cloned.1.call-update) | async-done | bytes 2883600 | tf_op jit(solution)/shard_map/all_gather | solution.py:84
  318.3 7.6 %convolution_convert_fusion.2 = bf16[768,2048]{1,0:T(8,128)(2,1)} fusion(bf16[2048,704]{0,1:T(8,128)(2,1)} %all-gather.11.cloned.1.call-done, f32[768,1408]{1,0:T(8,128)} %fusion.107), kind=kOutput, calls=%fused_computation.16 | convolution fusion | flops 2219409408 | bytes 10747904 | tf_op jit(solution)/shard_map/dot_general | solution.py:128
  325.9 36.7 %reduce-scatter.3.cloned.1.call-done = bf16[192,2048]{1,0:T(8,128)(2,1)} async-done(((bf16[768,2048]{1,0:T(8,128)(2,1)}), bf16[192,2048]{1,0:T(8,128)(2,1)}) %reduce-scatter.3.cloned.1.call-update) | async-done | bytes 786448 | tf_op jit(solution)/shard_map/reduce_scatter | solution.py:131
  362.6 19.6 %reduce-scatter.5.cloned.1.call-done = bf16[192,1024]{1,0:T(8,128)(2,1)} async-done(((bf16[192,2048]{1,0:T(8,128)(2,1)}), bf16[192,1024]{1,0:T(8,128)(2,1)}) %reduce-scatter.5.cloned.1.call-update) | async-done | bytes 393232 | tf_op jit(solution)/shard_map/reduce_scatter | solution.py:132
  382.3 1.9 add_convert_fusion
  (82 shorter events, 7.4 us)
Async XLA Ops:
  6.5 90.4 %copy-start = (bf16[1024,1024]{1,0:T(8,128)(2,1)S(1)}, bf16[1024,1024]{1,0:T(8,128)(2,1)}, u32[]{:S(2)}) copy-start(bf16[1024,1024]{1,0:T(8,128)(2,1)} %param.20) | copy-start | bytes 6291460
  6.5 6.2 %copy-start.10 = (bf16[192,1024]{1,0:T(8,128)(2,1)S(1)}, bf16[192,1024]{1,0:T(8,128)(2,1)}, u32[]{:S(2)}) copy-start(bf16[192,1024]{1,0:T(8,128)(2,1)} %param.13) | copy-start | bytes 1179652
  6.5 65.5 %copy-start.19 = (f32[256]{0:T(256)S(1)}, f32[256]{0:T(256)}, u32[]{:S(2)}) copy-start(f32[256]{0:T(256)} %param.17) | copy-start | bytes 3076
  6.5 65.5 %copy-start.17 = (bf16[256,512]{1,0:T(8,128)(2,1)S(1)}, bf16[256,512]{1,0:T(8,128)(2,1)}, u32[]{:S(2)}) copy-start(bf16[256,512]{1,0:T(8,128)(2,1)} %param.18) | copy-start | bytes 786436
  6.5 63.6 %all-gather.5.cloned.1.call-start = ((), (), s32[]{:S(2)}) async-start(), calls=%async_computation.4 | async-start | bytes 2433024 | tf_op jit(solution)/shard_map/all_gather | solution.py:69
  9.0 156.8 %all-gather.7.cloned.1.call-start = ((), (), s32[]{:S(2)}) async-start(), calls=%async_computation.5 | async-start | bytes 3932160 | tf_op jit(solution)/shard_map/all_gather | solution.py:124
  72.0 2.6 copy-start.14
  74.6 1.8 slice-start
  76.7 1.7 copy-start.7
  76.7 1.7 copy-start.13
  78.4 1.1 copy-start.6
  78.4 1.1 copy-start.12
  79.5 1.1 copy-start.5
  79.6 1.1 copy-start.11
  80.7 1.1 copy-start.4
  82.5 2.1 copy-start.3
  82.5 2.1 copy-start.15
  82.5 2.1 copy-start.18
  82.5 2.1 copy-start.20
  88.4 8.6 %copy-start.9 = (bf16[192,1024]{1,0:T(8,128)(2,1)S(1)}, bf16[192,1024]{1,0:T(8,128)(2,1)}, u32[]{:S(2)}) copy-start(bf16[192,1024]{1,0:T(8,128)(2,1)} %param.21) | copy-start | bytes 1179652
  97.0 12.8 %copy-start.16 = (f32[2048]{0:T(1024)S(1)}, f32[2048]{0:T(1024)}, u32[]{:S(2)}) copy-start(f32[2048]{0:T(1024)} %param.22) | copy-start | bytes 24580
  97.6 0.7 copy-start.1
  98.3 12.6 %copy-start.8 = (bf16[128,2816]{1,0:T(8,128)(2,1)S(1)}, bf16[128,2816]{1,0:T(8,128)(2,1)}, u32[]{:S(2)}) copy-start(bf16[128,2816]{1,0:T(8,128)(2,1)} %param.23) | copy-start | bytes 2162692
  110.9 148.5 %all-gather.9.cloned.1.call-start = ((), (), s32[]{:S(2)}) async-start(), calls=%async_computation.6 | async-start | bytes 7208960 | tf_op jit(solution)/shard_map/all_gather | solution.py:81
  150.3 168.0 %all-gather.11.cloned.1.call-start = ((), (), s32[]{:S(2)}) async-start(), calls=%async_computation.7 | async-start | bytes 3604480 | tf_op jit(solution)/shard_map/all_gather | solution.py:84
  165.7 196.9 %reduce-scatter.3.cloned.1.call-start = ((), (), s32[]{:S(2)}) async-start(), calls=%async_computation.8 | async-start | bytes 3932160 | tf_op jit(solution)/shard_map/reduce_scatter | solution.py:131
  325.9 56.4 %copy-start.2 = (bf16[192,1024]{1,0:T(8,128)(2,1)S(1)}, bf16[192,1024]{1,0:T(8,128)(2,1)}, u32[]{:S(2)}) copy-start(bf16[192,1024]{1,0:T(8,128)(2,1)} %copy-done.1) | copy-start | bytes 1179652
  325.9 56.4 %reduce-scatter.5.cloned.1.call-start = ((), (), s32[]{:S(2)}) async-start(), calls=%async_computation.9 | async-start | bytes 1179648 | tf_op jit(solution)/shard_map/reduce_scatter | solution.py:132
Sparse Core Ops, SparseCore 0:
  10.3 59.8 all-gather.4
  111.0 41.4 all-gather.6
  154.1 105.3 all-gather.8
  260.9 57.3 all-gather.10
  326.0 36.5 reduce-scatter.2
  364.7 17.4 reduce-scatter.4
